TPU v7x, 32 devices: a whole 2x2x4 slice. The times are simulated.
32 devices in a mesh: sp: 8 (over z, y), tp: 4 (over x, core).
Axes of the slice: x: 2, y: 2, z: 4, core: 2. Of those that a mesh axis runs over, the one named last changes fastest.
Arguments:
- arriving_hidden_state: bfloat16 [8192, 2048], P(('sp', 'tp')), may hold values from -6 to 6
- former_request_vectors: bfloat16 [8192, 1024], P('sp', 'tp'), may hold values from -6 to 6
- former_match_vectors: bfloat16 [8192, 1024], P('sp', 'tp'), may hold values from -6 to 6
- latter_request_vectors: bfloat16 [8192, 512], P('sp', 'tp'), may hold values from -6 to 6
- latter_match_vectors: bfloat16 [8192, 512], P('sp', 'tp'), may hold values from -6 to 6
- stored_vectors_both: bfloat16 [8192, 2, 1024], P('sp', None, 'tp'), may hold values from -6 to 6
- closing_valve_operands: bfloat16 [8192, 2, 1024], P('sp', None, 'tp'), may hold values from -6 to 6
- update_level_before_squash: bfloat16 [2, 8, 8192], P(None, 'tp', 'sp'), may hold values from -4 to -3
- fading_data_input: float32 [2, 8, 8192], P(None, 'tp', 'sp'), may hold values from -5.5 to 5.5
- sparse_fading_boost: float32 [2, 8, 8192], P(None, 'tp', 'sp'), may hold values from -2 to 0, as said below
- unitwise_fading_loglevel: float32 [2, 8], P(None, 'tp'), as said below
- fading_constant_term: float32 [2, 8], P(None, 'tp'), may hold values from -1 to 1
- unitwise_normalizer_coef: float32 [128], replicated, may hold values from 0.1 to 1.9
- emission_map_weights: bfloat16 [2048, 2048], replicated, may hold values from -0.125 to 0.125
- channel_normalizer_coef: float32 [2048], replicated, may hold values from 0.1 to 1.9
- switching_channel_map: bfloat16 [2048, 6144], P('sp', 'tp'), may hold values from -0.125 to 0.125
- broadening_channel_map: bfloat16 [2048, 6144], P('sp', 'tp'), may hold values from -0.125 to 0.125
- timewise_convolve_tapvalues: bfloat16 [3, 2, 6144], P(None, None, 'tp'), may hold values from -3.5 to 3.5
- narrowing_map_weights_in: bfloat16 [2048, 6144], P('sp', 'tp'), may hold values from -0.078125 to 0.078125
Outputs:
- mixed: bfloat16 [8192, 2048], P(('sp', 'tp'))
Inputs may be any that keep to these rules, and one draw needn't show every extreme that they name: `unitwise_fading_loglevel`: each entry is the logarithm of a per-position rate between 0.2 / 8192 and 2 / 64. `sparse_fading_boost`: zero except at three or fewer positions of the sequence.
All inputs are finite; a program needn't handle non-finite values.
Results may differ from a plain program's by a relative error of at most 0.015.
Values may be sent and summed in bfloat16 or wider, within the bound.
A program may use at most 128 MiB of HBM per device.

v0:
```python
import functools

import jax
import jax.numpy as jnp
from jax import lax
from jax.experimental import pallas as pl
from jax.experimental.pallas import tpu as pltpu
from jax.sharding import PartitionSpec as P

TAPS = 3
CHUNK = 128
BASE = 16
LANES = 128
EDGE = 16
UP, DOWN, ACROSS = 0, 1, 2

EPSILON = 1e-06
F32 = jnp.float32
BF16 = jnp.bfloat16
MESH = pl.DeviceIdType.MESH


def mm(a, b):
    return jnp.dot(a, b, preferred_element_type=F32)


def mm_nt(a, b):
    return lax.dot_general(a, b, (((1,), (1,)), ((), ())), preferred_element_type=F32)


def attend_heads(first, it, q_ref, k_ref, v_ref, cum_ref, gb_ref, heads, pm_ref, h0_ref, run_ref, last_ref):
    n = v_ref.shape[1] // CHUNK
    rows = lax.broadcasted_iota(jnp.int32, (CHUNK, CHUNK), 0)
    cols = lax.broadcasted_iota(jnp.int32, (CHUNK, CHUNK), 1)
    causal = rows >= cols
    eye = (rows == cols).astype(F32)
    lane = lax.broadcasted_iota(jnp.int32, (1, LANES), 1)
    narrow = it >= first
    other = jnp.maximum(it - first, 0)
    tile = jnp.where(narrow, first + other // 2, it)
    own = (lane // (LANES // 2) == other % 2) | jnp.logical_not(narrow)
    keep = jnp.where(own, 1.0, 0.0)
    diag = jnp.where(own, eye, 0.0)
    scale = jnp.where(narrow, (LANES // 2) ** -0.5, LANES ** -0.5)
    R = range(n)
    at = [pl.ds(c * CHUNK, CHUNK) for c in R]
    ks, qs, vs, low, intra, grown, fall, total, betas = ([None] * n for _ in range(9))
    for c in R:
        q = q_ref[tile, at[c], :].astype(F32) * keep
        k = k_ref[tile, at[c], :].astype(F32) * keep
        q = q * (lax.rsqrt(jnp.sum(q * q, axis=-1, keepdims=True) + EPSILON) * scale)
        k = k * lax.rsqrt(jnp.sum(k * k, axis=-1, keepdims=True) + EPSILON)
        cum = cum_ref[it, :, at[c]]
        beta = cum_ref[heads + it, :, at[c]]
        crow = jnp.broadcast_to(cum, (CHUNK, CHUNK))
        ccol = crow.T
        bcol = jnp.broadcast_to(beta, (CHUNK, CHUNK)).T
        total[c] = crow[:, CHUNK - 1:]
        decay = jnp.exp(jnp.where(causal, ccol - crow, -1e30))
        grown[c] = jnp.exp(ccol)
        kb = k.astype(BF16)
        kbeta = k * bcol
        both = mm_nt(jnp.concatenate([kbeta.astype(BF16), q.astype(BF16)], axis=0), kb)
        low[c] = jnp.where(rows > cols, both[:CHUNK] * decay, 0.0)
        intra[c] = (both[CHUNK:] * decay).astype(BF16)
        fall[c] = (k.T * jnp.exp(crow[:, CHUNK-1:] - crow)).astype(BF16)
        ks[c] = (kbeta * grown[c]).astype(BF16)
        vs[c] = (v_ref[it, at[c], :].astype(F32) * bcol).astype(BF16)
        qs[c] = q * grown[c]
    inner = (rows // BASE) == (cols // BASE)
    power = [jnp.where(inner, low[c], 0.0) for c in R]
    inv = [eye - power[c] for c in R]
    power = [p.astype(BF16) for p in power]
    size = 2
    while size < BASE:
        power = [mm(p, p).astype(BF16) for p in power]
        inv = [i + mm(i.astype(BF16), p) for i, p in zip(inv, power)]
        size *= 2
    block = BASE
    while block < CHUNK:
        here = ((rows // (2 * block)) == (cols // (2 * block))) & ((rows // block) != (cols // block))
        invb = [i.astype(BF16) for i in inv]
        half = [mm(invb[c], jnp.where(here, low[c], 0.0).astype(BF16)).astype(BF16) for c in R]
        inv = [inv[c] - mm(half[c], invb[c]) for c in R]
        block *= 2
    solved = [mm(inv[c].astype(BF16), jnp.concatenate([vs[c], ks[c]], axis=-1)).astype(BF16) for c in R]
    out = [mm(jnp.concatenate([fall[c], intra[c]], axis=0), solved[c]) for c in R]
    for c in R:
        h0_ref[it, at[c], :] = out[c][CHUNK:, :LANES]
        pm_ref[it, at[c], :] = (qs[c] - out[c][CHUNK:, LANES:]).astype(BF16)
    run = jnp.concatenate([jnp.zeros((LANES, LANES), F32), diag], axis=-1)
    for c in R:
        run_ref[it, c] = run.astype(BF16)
        cmap = (jnp.exp(total[c]) * diag - out[c][:CHUNK, LANES:]).astype(BF16)
        nxt = mm(cmap, run.astype(BF16))
        run = jnp.concatenate([nxt[:, :LANES] + out[c][:CHUNK, :LANES], nxt[:, LANES:]], axis=-1)
    last_ref[it] = run.astype(BF16)


def nearest(ring, place, rank):
    found = 0
    for here in range(ring):
        table = sorted(range(ring), key=lambda other: (abs(other - here), other))
        found = found + jnp.where(place == here, table[rank], 0)
    return found


def step_kernel(
    first,
    q1_ref, k1_ref, q2_ref, k2_ref, v_ref, valve_ref, emis_ref, skip_ref, gate_ref, up_ref, narrow_ref,
    gb_ref, coef_ref, norm_ref, taps_ref,
    out_ref,
    q_buf, k_buf, v_buf, valve_buf, cum_buf, pm_buf, h0_buf, run_buf, pair_buf, came_buf, went_buf, state_buf,
    att_buf, rows_buf, emis_buf, skip_buf, resid_buf, feats, gate_w, up_w, narrow_w, hidden,
    part_buf, half_buf, sum_buf, far_buf, out_buf,
    load_sem, own_sem, w_send, w_recv, pair_sem, chain_sem, att_send, att_recv, row_send, row_recv, halo_sem,
    half_send, half_recv, far_send, far_recv, out_sem,
):
    me, team_me = lax.axis_index("sp"), lax.axis_index("tp")
    spread, team = lax.axis_size("sp"), lax.axis_size("tp")
    ring, teams = spread // 2, team // 2
    place, side = me // 2, me % 2
    line, core = team_me // 2, team_me % 2
    length = v_buf.shape[1]
    chunks = length // CHUNK
    heads = v_buf.shape[0]
    width = feats.shape[1]
    share = length // team
    weights = (gate_w, up_w, narrow_w)
    block = gate_w.shape[0] // spread
    piece = block // 2
    started = []

    def go(wanted, make):
        if wanted is None:
            make().start()
        else:
            @pl.when(wanted)
            def _():
                make().start()

        started.append((wanted, make))

    def when(wanted, act):
        if wanted is None:
            act()
        else:
            pl.when(wanted)(act)

    loads = []

    def load(source, target):
        loads.append(pltpu.make_async_copy(source, target, load_sem.at[len(loads)]))
        loads[-1].start()

    own = []
    for which, ref in enumerate((gate_ref, up_ref, narrow_ref)):
        at = pl.ds(pl.multiple_of(me * block, block), block)
        own.append(pltpu.make_async_copy(ref, weights[which].at[at, :], own_sem.at[which]))
        own[-1].start()
    tiles = q_buf.shape[0]
    for tile in range(tiles):
        source = (q1_ref, k1_ref, tile) if tile < first else (q2_ref, k2_ref, tile - first)
        at = slice(source[2] * LANES, (source[2] + 1) * LANES)
        load(source[0].at[:, at], q_buf.at[tile])
        load(source[1].at[:, at], k_buf.at[tile])
    for head in range(heads):
        load(v_ref.at[:, head * LANES : (head + 1) * LANES], v_buf.at[head])
    early = len(loads)
    for head in range(heads):
        load(valve_ref.at[:, head * LANES : (head + 1) * LANES], valve_buf.at[head])
    middle = len(loads)
    load(skip_ref, skip_buf)
    load(emis_ref, emis_buf)

    barrier = pltpu.get_barrier_semaphore()
    for gap in (1, 2, spread - 2, spread - 1):
        pl.semaphore_signal(
            barrier, inc=1, device_id={"sp": lax.rem(me + gap, spread)}, device_id_type=MESH
        )
    for gap in range(1, team):
        pl.semaphore_signal(
            barrier, inc=1, device_id={"tp": lax.rem(team_me + gap, team)}, device_id_type=MESH
        )
    for one in own:
        one.wait()
    pl.semaphore_wait(barrier, 4 + team - 1)

    def block_copy(which, source, part, way):
        at = pl.ds(pl.multiple_of(source * block + part * piece, piece), piece)
        target = {UP: me + 2, DOWN: me - 2, ACROSS: me + 1 - 2 * side}[way]
        return pltpu.make_async_remote_copy(
            src_ref=weights[which].at[at, :],
            dst_ref=weights[which].at[at, :],
            send_sem=w_send.at[which, source, part, way],
            recv_sem=w_recv.at[which, source, part],
            device_id={"sp": target},
            device_id_type=MESH,
        )

    def send_line(which, part):
        go(place < ring - 1, lambda: block_copy(which, me, part, UP))
        go(place > 0, lambda: block_copy(which, me, part, DOWN))

    def send_across(which, part, rank):
        source = 2 * nearest(ring, place, rank) + side
        go(None, lambda: block_copy(which, source, part, ACROSS))

    def heard_across(which, part, rank):
        source = 2 * nearest(ring, place, rank) + 1 - side
        block_copy(which, source, part, ACROSS).wait_recv()

    def arrive(which, part, gap, held=None):
        low, high = me - 2 * gap, me + 2 * gap

        @pl.when(place >= gap)
        def _():
            block_copy(which, low, part, UP).wait_recv()

        @pl.when(place + gap < ring)
        def _():
            block_copy(which, high, part, DOWN).wait_recv()

        if gap < ring - 1:
            go((place + gap < ring) & (place > 0), lambda: block_copy(which, high, part, DOWN))
            onward = ((place >= gap) & (place < ring - 1), lambda: block_copy(which, low, part, UP))
            if held is None:
                go(*onward)
            else:
                held.append(onward)

    for which, part in ((0, 0), (0, 1), (1, 0)):
        send_across(which, part, 0)
        send_line(which, part)

    for chunk in range(chunks):
        at = slice(chunk * CHUNK, (chunk + 1) * CHUNK)
        level = gb_ref[:, at]
        cum = level
        lanes = lax.broadcasted_iota(jnp.int32, cum.shape, 1)
        shift = 1
        while shift < CHUNK:
            cum = cum + jnp.where(lanes >= shift, pltpu.roll(cum, shift, 1), 0.0)
            shift *= 2
        for head in range(heads):
            cum_buf[head, :, at] = cum[head : head + 1]
            cum_buf[heads + head, :, at] = level[heads + head : heads + head + 1]
    for one in loads[:early]:
        one.wait()

    def one_head(it, carry):
        attend_heads(
            first, it, q_buf, k_buf, v_buf, cum_buf, cum_buf, heads, pm_buf, h0_buf, run_buf,
            pair_buf.at[side],
        )
        return carry

    lax.fori_loop(0, heads, one_head, 0)

    def pair_copy():
        return pltpu.make_async_remote_copy(
            src_ref=pair_buf.at[side],
            dst_ref=pair_buf.at[side],
            send_sem=pair_sem.at[0],
            recv_sem=pair_sem.at[1],
            device_id={"sp": me + 1 - 2 * side},
            device_id_type=MESH,
        )

    go(None, pair_copy)
    send_across(1, 1, 0)
    send_line(1, 1)
    for one in loads[early:middle]:
        one.wait()
    pair_copy().wait_recv()
    held = []
    for part in range(2):
        arrive(0, part, 1, held)
        send_across(0, part, 1)

    def chain_copy():
        return pltpu.make_async_remote_copy(
            src_ref=went_buf,
            dst_ref=came_buf,
            send_sem=chain_sem.at[0],
            recv_sem=chain_sem.at[1],
            device_id={"sp": me + 2},
            device_id_type=MESH,
        )

    @pl.when(place == 0)
    def _():
        came_buf[...] = jnp.zeros_like(came_buf)

    @pl.when(place > 0)
    def _():
        chain_copy().wait_recv()

    before = [came_buf[head] for head in range(heads)]
    between = [
        mm(pair_buf[0, head, :, LANES:], before[head]) + pair_buf[0, head, :, :LANES].astype(F32)
        for head in range(heads)
    ]
    after = [
        mm(pair_buf[1, head, :, LANES:], between[head].astype(BF16))
        + pair_buf[1, head, :, :LANES].astype(F32)
        for head in range(heads)
    ]
    for head in range(heads):
        went_buf[head] = after[head].astype(BF16)
        state_buf[head] = jnp.where(side == 0, before[head].astype(F32), between[head]).astype(BF16)
    go(place < ring - 1, chain_copy)
    for onward in held:
        go(*onward)

    def finish(it, carry):
        coef = coef_ref[...]
        state = state_buf[it]
        starts = [
            (mm(run_buf[it, c, :, LANES:], state) + run_buf[it, c, :, :LANES].astype(F32)).astype(BF16)
            for c in range(chunks)
        ]
        lane = pl.ds(pl.multiple_of(it * LANES, LANES), LANES)
        for c in range(chunks):
            at = slice(c * CHUNK, (c + 1) * CHUNK)
            out = mm(pm_buf[it, at, :], starts[c]) + h0_buf[it, at, :]
            gate = valve_buf[it, at, :].astype(F32)
            scaled = out * lax.rsqrt(jnp.mean(out * out, axis=-1, keepdims=True) + EPSILON) * coef
            into, row = c * CHUNK // share, c * CHUNK % share
            att_buf[into, row : row + CHUNK, lane] = (
                scaled * (gate / (1.0 + jnp.exp(-gate)))
            ).astype(BF16)
        return carry

    lax.fori_loop(0, heads, finish, 0)

    mate = team_me + 1 - 2 * core
    others = []
    for gap in range(1, teams):
        there = lax.rem(line + gap, teams)
        others.append(2 * there + core)
        others.append(2 * there + 1 - core)

    def att_copy(source, target):
        return pltpu.make_async_remote_copy(
            src_ref=att_buf.at[target],
            dst_ref=rows_buf.at[source],
            send_sem=att_send.at[target],
            recv_sem=att_recv.at[source],
            device_id={"tp": target},
            device_id_type=MESH,
        )

    for peer in others + [mate]:
        go(None, functools.partial(att_copy, team_me, peer))
    for part in range(2):
        arrive(1, part, 1)
        send_across(1, part, 1)

    for one in loads[middle:]:
        one.wait()
    depth = rows_buf.shape[2] // 2

    def add_rows(x_ref, peer, start):
        for group in range(2):
            x = x_ref[:, group * depth : (group + 1) * depth]
            at = pl.ds(pl.multiple_of((group * team + peer) * depth, depth), depth)
            tile = min(512, width)
            for col in range(0, width, tile):
                base = (
                    skip_buf[:, col : col + tile].astype(F32)
                    if start and group == 0
                    else resid_buf[:, col : col + tile]
                )
                resid_buf[:, col : col + tile] = base + mm(x, emis_buf[at, col : col + tile])

    add_rows(att_buf.at[team_me], team_me, True)
    for peer in [mate] + others:
        att_copy(peer, team_me).wait_recv()
        add_rows(rows_buf.at[peer], peer, False)
    mine = pl.multiple_of(EDGE + team_me * share, EDGE)
    step = min(64, share)
    for row in range(0, share, step):
        total = resid_buf[row : row + step, :]
        scale = lax.rsqrt(jnp.mean(total * total, axis=-1, keepdims=True) + EPSILON)
        feats[pl.ds(mine + row, step), :] = (total * scale * norm_ref[...]).astype(BF16)

    row_part = share // 2

    def row_copy(source, target, part, slot):
        at = pl.ds(pl.multiple_of(EDGE + source * share + part * row_part, EDGE), row_part)
        return pltpu.make_async_remote_copy(
            src_ref=feats.at[at, :],
            dst_ref=feats.at[at, :],
            send_sem=row_send.at[slot, part],
            recv_sem=row_recv.at[source, part],
            device_id={"tp": target},
            device_id_type=MESH,
        )

    far = [2 * lax.rem(line + gap, teams) + core for gap in range(1, teams)]
    for part in range(2):
        for slot, peer in enumerate(far):
            go(None, functools.partial(row_copy, team_me, peer, part, 2 * slot + 1))
    for part in range(2):
        go(None, functools.partial(row_copy, team_me, mate, part, 0))
    for part in range(2):
        if ring > 2:
            arrive(0, part, 2)
            send_across(0, part, 2)
    for part in range(2):
        for slot, peer in enumerate(far):
            row_copy(peer, team_me, part, 0).wait_recv()
            go(None, functools.partial(row_copy, peer, mate, part, 2 * slot + 2))
    for part in range(2):
        row_copy(mate, team_me, part, 0).wait_recv()
        for peer in far:
            row_copy(peer + 1 - 2 * core, team_me, part, 0).wait_recv()

    def halo_copy():
        return pltpu.make_async_remote_copy(
            src_ref=feats.at[length:, :],
            dst_ref=feats.at[:EDGE, :],
            send_sem=halo_sem.at[0],
            recv_sem=halo_sem.at[1],
            device_id={"sp": me + 1},
            device_id_type=MESH,
        )

    go(me < spread - 1, halo_copy)

    @pl.when(me == 0)
    def _():
        feats[:EDGE, :] = jnp.zeros((EDGE, width), BF16)

    for part in range(2):
        if ring > 2:
            arrive(1, part, 2)
            send_across(1, part, 2)
    for part in range(2):
        send_line(2, part)
    for gap in range(3, ring):
        for which in range(2):
            for part in range(2):
                arrive(which, part, gap)
                send_across(which, part, gap)
    for part in range(2):
        send_across(2, part, 0)
    for part in range(2):
        arrive(2, part, 1)
        send_across(2, part, 1)
    for rank in range(ring):
        for which in range(2):
            for part in range(2):
                heard_across(which, part, rank)

    @pl.when(me > 0)
    def _():
        halo_copy().wait_recv()

    units = hidden.shape[1]
    wide = min(256, units)
    tall = min(512, length)
    turns = units // wide * (length // tall)

    def hidden_tile(turn, carry):
        col = pl.ds(pl.multiple_of(turn // (length // tall) * wide, wide), wide)
        row = pl.multiple_of(turn % (length // tall) * tall, tall)
        x = feats[pl.ds(row, tall + EDGE), :]
        taken = []
        for which in range(2):
            low = mm(x, weights[which][:, col]).astype(BF16).astype(F32)
            total = 0.0
            for tap in range(TAPS):
                moved = low[EDGE - TAPS + 1 + tap : EDGE - TAPS + 1 + tap + tall]
                total = total + taps_ref[2 * tap + which : 2 * tap + which + 1, col] * moved
            taken.append(total)
        gate, up = taken
        hidden[pl.ds(row, tall), col] = (gate / (1.0 + jnp.exp(-gate)) * up).astype(BF16)
        return carry

    cuts = [turns * cut // (ring - 1) for cut in range(ring)]
    for cut in range(ring - 1):
        lax.fori_loop(cuts[cut], cuts[cut + 1], hidden_tile, 0)
        gap = cut + 2
        if gap < ring:
            for part in range(2):
                arrive(2, part, gap)
                send_across(2, part, gap)

    def owner(turn):
        rank = nearest(ring, place, turn % ring)
        return 2 * rank + (side if turn < ring else 1 - side)

    def half_copy(turn, there):
        at = pl.ds(pl.multiple_of((2 * there + 1 - core) * share, share), share)
        return pltpu.make_async_remote_copy(
            src_ref=part_buf.at[turn, at, :],
            dst_ref=half_buf.at[turn, there],
            send_sem=half_send.at[turn, there],
            recv_sem=half_recv.at[turn, there],
            device_id={"tp": mate},
            device_id_type=MESH,
        )

    def far_copy(turn, there, source):
        return pltpu.make_async_remote_copy(
            src_ref=sum_buf.at[turn, there],
            dst_ref=far_buf.at[turn, source],
            send_sem=far_send.at[turn, there],
            recv_sem=far_recv.at[turn, source],
            device_id={"tp": 2 * there + core},
            device_id_type=MESH,
        )

    def both(turn, there):
        at = pl.ds(pl.multiple_of((2 * there + core) * share, share), share)
        return part_buf[turn, at, :].astype(F32) + half_buf[turn, there].astype(F32)

    def product(turn):
        source = owner(turn)
        if turn >= ring:
            for part in range(2):
                heard_across(2, part, turn % ring)
        at = pl.ds(pl.multiple_of(source * block, block), block)
        part_buf[turn] = mm_nt(hidden[...], narrow_w[at, :]).astype(BF16)
        for there in range(teams):
            go(None, functools.partial(half_copy, turn, there))

    def pass_on(turn):
        for there in range(teams):
            half_copy(turn, there).wait_recv()
        for gap in range(1, teams):
            there = lax.rem(line + gap, teams)
            sum_buf[turn, there] = both(turn, there).astype(BF16)
            go(None, functools.partial(far_copy, turn, there, line))

    def close(turn):
        col = pl.ds(pl.multiple_of(owner(turn) * block, block), block)
        total = resid_buf[:, col] + both(turn, line)
        for gap in range(1, teams):
            there = lax.rem(line + gap, teams)
            far_copy(turn, line, there).wait_recv()
            total = total + far_buf[turn, there].astype(F32)
        out_buf[:, col] = total.astype(BF16)
        put(turn).start()

    def put(turn):
        col = pl.ds(pl.multiple_of(owner(turn) * block, block), block)
        return pltpu.make_async_copy(out_buf.at[:, col], out_ref.at[:, col], out_sem.at[turn])

    for turn in range(spread + 2):
        if turn < spread:
            product(turn)
        if 1 <= turn <= spread:
            pass_on(turn - 1)
        if turn >= 2:
            close(turn - 2)
    for turn in range(spread):
        put(turn).wait()
    for wanted, make in started:
        when(wanted, lambda make=make: make().wait_send())


def whole_step(first, q1, k1, q2, k2, v, valve, emis, skip, gate, up, narrow, gb, coef, norm, taps):
    spread, team = lax.axis_size("sp"), lax.axis_size("tp")
    teams = team // 2
    length = q1.shape[0]
    heads = v.shape[1] // LANES
    chunks = length // CHUNK
    tiles = (q1.shape[1] + q2.shape[1]) // LANES
    share, width = skip.shape
    block, units = gate.shape
    anywhere = pl.BlockSpec(memory_space=pl.ANY)
    inside = pl.BlockSpec(memory_space=pltpu.VMEM)
    dma = pltpu.SemaphoreType.DMA

    def vmem(*shape, dtype=BF16):
        return pltpu.VMEM(shape, dtype)

    scratch = [
        vmem(tiles, length, LANES),
        vmem(tiles, length, LANES),
        vmem(heads, length, LANES),
        vmem(heads, length, LANES),
        vmem(2 * heads, 1, length, dtype=F32),
        vmem(heads, length, LANES),
        vmem(heads, length, LANES, dtype=F32),
        vmem(heads, chunks, LANES, 2 * LANES),
        vmem(2, heads, LANES, 2 * LANES),
        vmem(heads, LANES, LANES),
        vmem(heads, LANES, LANES),
        vmem(heads, LANES, LANES),
        vmem(team, share, heads * LANES),
        vmem(team, share, heads * LANES),
        vmem(*emis.shape),
        vmem(share, width),
        vmem(share, width, dtype=F32),
        vmem(EDGE + length, width),
        vmem(width, units),
        vmem(width, units),
        vmem(width, units),
        vmem(length, units),
        vmem(spread, length, block),
        vmem(spread, teams, share, block),
        vmem(spread, teams, share, block),
        vmem(spread, teams, share, block),
        vmem(share, width),
        dma((2 * tiles + 2 * heads + 2,)),
        dma((3,)),
        dma((3, spread, 2, 3)),
        dma((3, spread, 2)),
        dma((2,)),
        dma((2,)),
        dma((team,)),
        dma((team,)),
        dma((2 * teams, 2)),
        dma((team, 2)),
        dma((2,)),
        dma((spread, teams)),
        dma((spread, teams)),
        dma((spread, teams)),
        dma((spread, teams)),
        dma((spread,)),
    ]
    return pl.pallas_call(
        functools.partial(step_kernel, first),
        in_specs=[anywhere] * 11 + [inside] * 4,
        out_specs=anywhere,
        out_shape=jax.ShapeDtypeStruct((share, width), BF16),
        scratch_shapes=scratch,
        compiler_params=pltpu.CompilerParams(
            collective_id=1, has_side_effects=True, vmem_limit_bytes=67043328
        ),
        cost_estimate=pl.CostEstimate(flops=10**11, bytes_accessed=10**8, transcendentals=0),
    )(q1, k1, q2, k2, v, valve, emis, skip, gate, up, narrow, gb, coef, norm, taps)


def per_device(
    arriving_hidden_state,
    former_request_vectors,
    former_match_vectors,
    latter_request_vectors,
    latter_match_vectors,
    stored_vectors_both,
    closing_valve_operands,
    update_level_before_squash,
    fading_data_input,
    sparse_fading_boost,
    unitwise_fading_loglevel,
    fading_constant_term,
    unitwise_normalizer_coef,
    emission_map_weights,
    channel_normalizer_coef,
    switching_channel_map,
    broadening_channel_map,
    timewise_convolve_tapvalues,
    narrowing_map_weights_in,
):
    length = former_request_vectors.shape[0]
    level = (
        -jnp.exp(unitwise_fading_loglevel)[..., None]
        * jax.nn.softplus(fading_data_input + fading_constant_term[..., None])
        + sparse_fading_boost
    )
    beta_rate = jax.nn.sigmoid(update_level_before_squash.astype(jnp.float32))
    gates_beta = jnp.concatenate([level, beta_rate], axis=0).reshape(-1, length)
    gates_beta = jnp.pad(gates_beta, ((0, -gates_beta.shape[0] % 8), (0, 0)))
    spare = -latter_request_vectors.shape[1] % LANES
    return whole_step(
        former_request_vectors.shape[1] // LANES,
        former_request_vectors,
        former_match_vectors,
        jnp.pad(latter_request_vectors, ((0, 0), (0, spare))),
        jnp.pad(latter_match_vectors, ((0, 0), (0, spare))),
        stored_vectors_both.reshape(length, -1),
        closing_valve_operands.reshape(length, -1),
        emission_map_weights,
        arriving_hidden_state,
        switching_channel_map,
        broadening_channel_map,
        narrowing_map_weights_in,
        gates_beta,
        unitwise_normalizer_coef.reshape(1, -1),
        channel_normalizer_coef.reshape(1, -1),
        timewise_convolve_tapvalues.astype(F32).reshape(2 * TAPS, -1),
    )


def solution(mesh):
    placed = (
        P(("sp", "tp"), None),
        P("sp", "tp"),
        P("sp", "tp"),
        P("sp", "tp"),
        P("sp", "tp"),
        P("sp", None, "tp"),
        P("sp", None, "tp"),
        P(None, "tp", "sp"),
        P(None, "tp", "sp"),
        P(None, "tp", "sp"),
        P(None, "tp"),
        P(None, "tp"),
        P(),
        P(),
        P(),
        P("sp", "tp"),
        P("sp", "tp"),
        P(None, None, "tp"),
        P("sp", "tp"),
    )
    return jax.shard_map(
        per_device, mesh=mesh, in_specs=placed, out_specs=P(("sp", "tp"), None), check_vma=False
    )
```

profile of v0, /device:TPU:28, one launch (start us, length us, event | category | flops | bytes accessed | tf_op | source)
XLA Modules:
  0.0 237.8 jit_solution(203854698903746908)
XLA Ops:
  0.0 0.7 exponential_negate_fusion
  0.7 0.9 fusion.1
  1.6 0.6 reshape.25.gb_ref
  2.2 1.3 reshape.31.taps_ref
  3.5 2.4 %copy.20 = bf16[128,8,2,256]{3,1,2,0:T(8,128)(2,1)} copy(bf16[128,8,2,256]{3,2,1,0:T(2,128)(2,1)} %bitcast.6) | data formatting | bytes 2097152
  6.0 2.4 %copy.21 = bf16[128,8,2,256]{3,1,2,0:T(8,128)(2,1)} copy(bf16[128,8,2,256]{3,2,1,0:T(2,128)(2,1)} %bitcast.7) | data formatting | bytes 2097152
  8.4 227.1 %shard_map.181 = bf16[256,2048]{1,0:T(8,128)(2,1)} custom-call(bf16[1024,256]{1,0:T(8,128)(2,1)} %q1_ref.1, bf16[1024,256]{1,0:T(8,128)(2,1)} %k1_ref.1, bf16[1024,128]{1,0:T(8,128)(2,1)} %q2_ref.1, bf16[1024,128]{1,0:T(8,128)(2,1)} %k2_ref.1, bf16[1024,512]{1,0:T(8,128)(2,1)} %bitcast.8, bf16[1024,512]{1,0:T(8,128)(2,1)} %bitcast.9, ...), custom_call_target="tpu_custom_call" | custom-call | flops 99999997952 | bytes 100000000 | tf_op jit(solution)/shard_map/pallas_call | solution.py:626
  235.5 2.3 copy.23
  (1 shorter events, 0.0 us)
where the time goes:
time: 240 us; the launch traced here: 238 us
  Pallas kernels  227 us (95%)
  local copies, waits for them, and re-layouts  9.13 us (4%)
    pallas_call x1, Pallas kernels, whole_step(): pl.pallas_call(functools.partial(step_kernel, first), in_specs=[anywhere]...  227 us
    unnamed x3, local copies, waits for them, and re-layouts  7.16 us

commit v1 on v0

--- a/solution.py
+++ b/solution.py
@@ -110,9 +110,9 @@
     q1_ref, k1_ref, q2_ref, k2_ref, v_ref, valve_ref, emis_ref, skip_ref, gate_ref, up_ref, narrow_ref,
     gb_ref, coef_ref, norm_ref, taps_ref,
     out_ref,
-    q_buf, k_buf, v_buf, valve_buf, cum_buf, pm_buf, h0_buf, run_buf, pair_buf, came_buf, went_buf, state_buf,
+    q_buf, k_buf, v_buf, valve_buf, v_raw, valve_raw, cum_buf, pm_buf, h0_buf, run_buf, pair_buf, came_buf, went_buf, state_buf,
     att_buf, rows_buf, emis_buf, skip_buf, resid_buf, feats, gate_w, up_w, narrow_w, hidden,
-    part_buf, half_buf, sum_buf, far_buf, out_buf,
+    half_buf, far_buf, out_buf,
     load_sem, own_sem, w_send, w_recv, pair_sem, chain_sem, att_send, att_recv, row_send, row_recv, halo_sem,
     half_send, half_recv, far_send, far_recv, out_sem,
 ):
@@ -128,7 +128,8 @@
     share = length // team
     weights = (gate_w, up_w, narrow_w)
     block = gate_w.shape[0] // spread
-    piece = block // 2
+    units = gate_w.shape[1]
+    partner = me + 1 - 2 * side
     started = []
 
     def go(wanted, make):
@@ -156,7 +157,8 @@
     own = []
     for which, ref in enumerate((gate_ref, up_ref, narrow_ref)):
         at = pl.ds(pl.multiple_of(me * block, block), block)
-        own.append(pltpu.make_async_copy(ref, weights[which].at[at, :], own_sem.at[which]))
+        col = pl.ds(pl.multiple_of(side * units, LANES), units)
+        own.append(pltpu.make_async_copy(ref.at[:, col], weights[which].at[at, :], own_sem.at[which]))
         own[-1].start()
     tiles = q_buf.shape[0]
     for tile in range(tiles):
@@ -164,19 +166,35 @@
         at = slice(source[2] * LANES, (source[2] + 1) * LANES)
         load(source[0].at[:, at], q_buf.at[tile])
         load(source[1].at[:, at], k_buf.at[tile])
-    for head in range(heads):
-        load(v_ref.at[:, head * LANES : (head + 1) * LANES], v_buf.at[head])
+    load(v_ref, v_raw)
     early = len(loads)
-    for head in range(heads):
-        load(valve_ref.at[:, head * LANES : (head + 1) * LANES], valve_buf.at[head])
+    load(valve_ref, valve_raw)
     middle = len(loads)
+
+    def by_head(raw, into):
+        def turn(c, carry):
+            at = pl.ds(pl.multiple_of(c * CHUNK, CHUNK), CHUNK)
+            rows = raw[at, :, :].astype(F32)
+            for head in range(heads):
+                group, here = head // (heads // 2), head % (heads // 2)
+                into[head, at, :] = rows[:, group, here * LANES : (here + 1) * LANES].astype(BF16)
+            return carry
+
+        lax.fori_loop(0, chunks, turn, 0)
     load(skip_ref, skip_buf)
     load(emis_ref, emis_buf)
 
     barrier = pltpu.get_barrier_semaphore()
-    for gap in (1, 2, spread - 2, spread - 1):
+    for gap in (2, spread - 2):
         pl.semaphore_signal(
             barrier, inc=1, device_id={"sp": lax.rem(me + gap, spread)}, device_id_type=MESH
+        )
+    for there in range(teams):
+        pl.semaphore_signal(
+            barrier,
+            inc=1,
+            device_id={"sp": partner, "tp": 2 * there + core},
+            device_id_type=MESH,
         )
     for gap in range(1, team):
         pl.semaphore_signal(
@@ -184,34 +202,46 @@
         )
     for one in own:
         one.wait()
-    pl.semaphore_wait(barrier, 4 + team - 1)
-
-    def block_copy(which, source, part, way):
-        at = pl.ds(pl.multiple_of(source * block + part * piece, piece), piece)
-        target = {UP: me + 2, DOWN: me - 2, ACROSS: me + 1 - 2 * side}[way]
+    pl.semaphore_wait(barrier, 2 + teams + team - 1)
+
+    def owner(there, part):
+        return 2 * there + (side if part == 0 else 1 - side)
+
+    def block_copy(which, there, part, way):
+        source = owner(there, part)
+        at = pl.ds(pl.multiple_of(source * block, block), block)
         return pltpu.make_async_remote_copy(
             src_ref=weights[which].at[at, :],
             dst_ref=weights[which].at[at, :],
-            send_sem=w_send.at[which, source, part, way],
-            recv_sem=w_recv.at[which, source, part],
-            device_id={"sp": target},
-            device_id_type=MESH,
-        )
+            send_sem=w_send.at[which, source, way],
+            recv_sem=w_recv.at[which, source],
+            device_id={"sp": me + 2 if way == UP else me - 2},
+            device_id_type=MESH,
+        )
+
+    def across_copy(which, source):
+        at = pl.ds(pl.multiple_of(source * block, block), block)
+        col = pl.ds(pl.multiple_of((1 - side) * units, LANES), units)
+        return pltpu.make_async_remote_copy(
+            src_ref=(gate_ref, up_ref, narrow_ref)[which].at[:, col],
+            dst_ref=weights[which].at[at, :],
+            send_sem=w_send.at[which, source, ACROSS],
+            recv_sem=w_recv.at[which, source],
+            device_id={"sp": partner},
+            device_id_type=MESH,
+        )
+
+    def send_across(which):
+        go(None, lambda: across_copy(which, me))
 
     def send_line(which, part):
-        go(place < ring - 1, lambda: block_copy(which, me, part, UP))
-        go(place > 0, lambda: block_copy(which, me, part, DOWN))
-
-    def send_across(which, part, rank):
-        source = 2 * nearest(ring, place, rank) + side
-        go(None, lambda: block_copy(which, source, part, ACROSS))
-
-    def heard_across(which, part, rank):
-        source = 2 * nearest(ring, place, rank) + 1 - side
-        block_copy(which, source, part, ACROSS).wait_recv()
+        if part:
+            across_copy(which, partner).wait_recv()
+        go(place < ring - 1, lambda: block_copy(which, place, part, UP))
+        go(place > 0, lambda: block_copy(which, place, part, DOWN))
 
     def arrive(which, part, gap, held=None):
-        low, high = me - 2 * gap, me + 2 * gap
+        low, high = place - gap, place + gap
 
         @pl.when(place >= gap)
         def _():
@@ -223,15 +253,18 @@
 
         if gap < ring - 1:
             go((place + gap < ring) & (place > 0), lambda: block_copy(which, high, part, DOWN))
-            onward = ((place >= gap) & (place < ring - 1), lambda: block_copy(which, low, part, UP))
+            wanted = (place >= gap) & (place < ring - 1)
+            make = lambda: block_copy(which, low, part, UP)
             if held is None:
-                go(*onward)
+                go(wanted, make)
             else:
-                held.append(onward)
-
-    for which, part in ((0, 0), (0, 1), (1, 0)):
-        send_across(which, part, 0)
-        send_line(which, part)
+                go(wanted & (place == ring - 2), make)
+                held.append((wanted & (place < ring - 2), make))
+
+    for which in range(2):
+        send_across(which)
+        send_line(which, 0)
+    send_line(2, 0)
 
     for chunk in range(chunks):
         at = slice(chunk * CHUNK, (chunk + 1) * CHUNK)
@@ -247,6 +280,7 @@
             cum_buf[heads + head, :, at] = level[heads + head : heads + head + 1]
     for one in loads[:early]:
         one.wait()
+    by_head(v_raw, v_buf)
 
     def one_head(it, carry):
         attend_heads(
@@ -263,20 +297,21 @@
             dst_ref=pair_buf.at[side],
             send_sem=pair_sem.at[0],
             recv_sem=pair_sem.at[1],
-            device_id={"sp": me + 1 - 2 * side},
+            device_id={"sp": partner},
             device_id_type=MESH,
         )
 
     go(None, pair_copy)
-    send_across(1, 1, 0)
-    send_line(1, 1)
+    send_across(2)
+    for which in range(2):
+        send_line(which, 1)
+    held = []
+    if ring > 1:
+        arrive(0, 0, 1, held)
     for one in loads[early:middle]:
         one.wait()
+    by_head(valve_raw, valve_buf)
     pair_copy().wait_recv()
-    held = []
-    for part in range(2):
-        arrive(0, part, 1, held)
-        send_across(0, part, 1)
 
     def chain_copy():
         return pltpu.make_async_remote_copy(
@@ -312,6 +347,7 @@
     go(place < ring - 1, chain_copy)
     for onward in held:
         go(*onward)
+    arrive(1, 0, 1)
 
     def finish(it, carry):
         coef = coef_ref[...]
@@ -353,9 +389,11 @@
 
     for peer in others + [mate]:
         go(None, functools.partial(att_copy, team_me, peer))
-    for part in range(2):
-        arrive(1, part, 1)
-        send_across(1, part, 1)
+    arrive(0, 1, 1)
+    arrive(1, 1, 1)
+    for which in range(2):
+        if ring > 2:
+            arrive(which, 0, 2)
 
     for one in loads[middle:]:
         one.wait()
@@ -378,7 +416,8 @@
     for peer in [mate] + others:
         att_copy(peer, team_me).wait_recv()
         add_rows(rows_buf.at[peer], peer, False)
-    mine = pl.multiple_of(EDGE + team_me * share, EDGE)
+    here = side * team + team_me
+    mine = pl.multiple_of(EDGE + here * share, EDGE)
     step = min(64, share)
     for row in range(0, share, step):
         total = resid_buf[row : row + step, :]
@@ -387,175 +426,213 @@
 
     row_part = share // 2
 
-    def row_copy(source, target, part, slot):
+    def row_copy(source, part, way, target):
         at = pl.ds(pl.multiple_of(EDGE + source * share + part * row_part, EDGE), row_part)
         return pltpu.make_async_remote_copy(
             src_ref=feats.at[at, :],
             dst_ref=feats.at[at, :],
-            send_sem=row_send.at[slot, part],
+            send_sem=row_send.at[source, part, way],
             recv_sem=row_recv.at[source, part],
-            device_id={"tp": target},
-            device_id_type=MESH,
-        )
-
-    far = [2 * lax.rem(line + gap, teams) + core for gap in range(1, teams)]
+            device_id=target,
+            device_id_type=MESH,
+        )
+
+    def row_index(group, there, lane):
+        return group * team + 2 * there + lane
+
+    def row_arrive(source, part):
+        row_copy(source, part, 0, {"tp": mate}).wait_recv()
+
+    def row_send_to(source, part, way, target):
+        go(None, lambda: row_copy(source, part, way, target))
+
+    aside = [lax.rem(line + gap, teams) for gap in range(1, teams)]
     for part in range(2):
-        for slot, peer in enumerate(far):
-            go(None, functools.partial(row_copy, team_me, peer, part, 2 * slot + 1))
+        for gap, there in enumerate(aside):
+            row_send_to(here, part, 2 + gap, {"tp": 2 * there + core})
+        row_send_to(here, part, 1, {"sp": partner})
     for part in range(2):
-        go(None, functools.partial(row_copy, team_me, mate, part, 0))
+        row_send_to(here, part, 0, {"tp": mate})
+    for which in range(2):
+        if ring > 2:
+            arrive(which, 1, 2)
+    send_line(2, 1)
+    beyond = row_index(1 - side, line, core)
+    row_arrive(beyond, 0)
+    for gap, there in enumerate(aside):
+        row_send_to(beyond, 0, 2 + gap, {"tp": 2 * there + core})
+    row_send_to(beyond, 0, 0, {"tp": mate})
+    for there in aside:
+        row_arrive(row_index(side, there, core), 0)
+        row_send_to(row_index(side, there, core), 0, 0, {"tp": mate})
+    for there in aside:
+        row_arrive(row_index(side, there, core), 1)
+        row_send_to(row_index(side, there, core), 1, 1, {"sp": partner})
+        row_send_to(row_index(side, there, core), 1, 0, {"tp": mate})
+    row_arrive(beyond, 1)
+    row_send_to(beyond, 1, 0, {"tp": mate})
+    for there in aside:
+        for part in range(2):
+            row_arrive(row_index(1 - side, there, core), part)
+            row_send_to(row_index(1 - side, there, core), part, 0, {"tp": mate})
     for part in range(2):
-        if ring > 2:
-            arrive(0, part, 2)
-            send_across(0, part, 2)
-    for part in range(2):
-        for slot, peer in enumerate(far):
-            row_copy(peer, team_me, part, 0).wait_recv()
-            go(None, functools.partial(row_copy, peer, mate, part, 2 * slot + 2))
-    for part in range(2):
-        row_copy(mate, team_me, part, 0).wait_recv()
-        for peer in far:
-            row_copy(peer + 1 - 2 * core, team_me, part, 0).wait_recv()
+        for group in range(2):
+            for there in range(teams):
+                row_arrive(row_index(group, there, 1 - core), part)
 
     def halo_copy():
         return pltpu.make_async_remote_copy(
-            src_ref=feats.at[length:, :],
+            src_ref=feats.at[2 * length :, :],
             dst_ref=feats.at[:EDGE, :],
             send_sem=halo_sem.at[0],
             recv_sem=halo_sem.at[1],
-            device_id={"sp": me + 1},
-            device_id_type=MESH,
-        )
-
-    go(me < spread - 1, halo_copy)
-
-    @pl.when(me == 0)
+            device_id={"sp": me + 2},
+            device_id_type=MESH,
+        )
+
+    go(place < ring - 1, halo_copy)
+
+    @pl.when(place == 0)
     def _():
         feats[:EDGE, :] = jnp.zeros((EDGE, width), BF16)
 
-    for part in range(2):
-        if ring > 2:
-            arrive(1, part, 2)
-            send_across(1, part, 2)
-    for part in range(2):
-        send_line(2, part)
     for gap in range(3, ring):
-        for which in range(2):
-            for part in range(2):
+        for part in range(2):
+            for which in range(2):
                 arrive(which, part, gap)
-                send_across(which, part, gap)
-    for part in range(2):
-        send_across(2, part, 0)
-    for part in range(2):
-        arrive(2, part, 1)
-        send_across(2, part, 1)
-    for rank in range(ring):
-        for which in range(2):
-            for part in range(2):
-                heard_across(which, part, rank)
-
-    @pl.when(me > 0)
+    arrive(2, 0, 1)
+
+    @pl.when(place > 0)
     def _():
         halo_copy().wait_recv()
 
-    units = hidden.shape[1]
-    wide = min(256, units)
-    tall = min(512, length)
-    turns = units // wide * (length // tall)
-
-    def hidden_tile(turn, carry):
-        col = pl.ds(pl.multiple_of(turn // (length // tall) * wide, wide), wide)
-        row = pl.multiple_of(turn % (length // tall) * tall, tall)
-        x = feats[pl.ds(row, tall + EDGE), :]
-        taken = []
-        for which in range(2):
-            low = mm(x, weights[which][:, col]).astype(BF16).astype(F32)
-            total = 0.0
-            for tap in range(TAPS):
-                moved = low[EDGE - TAPS + 1 + tap : EDGE - TAPS + 1 + tap + tall]
-                total = total + taps_ref[2 * tap + which : 2 * tap + which + 1, col] * moved
-            taken.append(total)
-        gate, up = taken
-        hidden[pl.ds(row, tall), col] = (gate / (1.0 + jnp.exp(-gate)) * up).astype(BF16)
-        return carry
-
-    cuts = [turns * cut // (ring - 1) for cut in range(ring)]
-    for cut in range(ring - 1):
-        lax.fori_loop(cuts[cut], cuts[cut + 1], hidden_tile, 0)
-        gap = cut + 2
-        if gap < ring:
-            for part in range(2):
-                arrive(2, part, gap)
-                send_across(2, part, gap)
-
-    def owner(turn):
-        rank = nearest(ring, place, turn % ring)
-        return 2 * rank + (side if turn < ring else 1 - side)
-
-    def half_copy(turn, there):
-        at = pl.ds(pl.multiple_of((2 * there + 1 - core) * share, share), share)
-        return pltpu.make_async_remote_copy(
-            src_ref=part_buf.at[turn, at, :],
-            dst_ref=half_buf.at[turn, there],
-            send_sem=half_send.at[turn, there],
-            recv_sem=half_recv.at[turn, there],
+    wide = 256 if units % 256 == 0 else LANES
+    tall = 2 * share
+
+    def hidden_rows(row):
+        def tile(turn, carry):
+            col = pl.ds(pl.multiple_of(turn * wide, wide), wide)
+            tap_col = pl.ds(pl.multiple_of(side * units + turn * wide, LANES), wide)
+            x = feats[pl.ds(row, tall + EDGE), :]
+            taken = []
+            for which in range(2):
+                low = mm(x, weights[which][:, col]).astype(BF16).astype(F32)
+                total = 0.0
+                for tap in range(TAPS):
+                    moved = low[EDGE - TAPS + 1 + tap : EDGE - TAPS + 1 + tap + tall]
+                    total = total + taps_ref[2 * tap + which : 2 * tap + which + 1, tap_col] * moved
+                taken.append(total)
+            gate, up = taken
+            hidden[pl.ds(row, tall), col] = (gate / (1.0 + jnp.exp(-gate)) * up).astype(BF16)
+            return carry
+
+        lax.fori_loop(0, units // wide, tile, 0)
+
+    part_buf = emis_buf
+    early_turns = range(min(3, spread))
+    seen = {(0, 1)}
+    chips = [(ds, dl) for ds in range(2) for dl in range(teams)]
+
+    def chip(ds, dl):
+        return (side + ds) % 2, lax.rem(line + dl, teams)
+
+    def chip_at(ds, dl):
+        group, there = chip(ds, dl)
+        return group * teams + there
+
+    def rows_of(ds, dl, lane):
+        group, there = chip(ds, dl)
+        return pl.ds(pl.multiple_of(row_index(group, there, lane) * share, share), share)
+
+    def half_copy(turn, ds, dl):
+        return pltpu.make_async_remote_copy(
+            src_ref=part_buf.at[rows_of(ds, dl, 1 - core), turn * block : (turn + 1) * block],
+            dst_ref=half_buf.at[turn, chip_at(ds, dl)],
+            send_sem=half_send.at[turn, chip_at(ds, dl)],
+            recv_sem=half_recv.at[turn, chip_at(ds, dl)],
             device_id={"tp": mate},
             device_id_type=MESH,
         )
 
-    def far_copy(turn, there, source):
-        return pltpu.make_async_remote_copy(
-            src_ref=sum_buf.at[turn, there],
-            dst_ref=far_buf.at[turn, source],
-            send_sem=far_send.at[turn, there],
-            recv_sem=far_recv.at[turn, source],
-            device_id={"tp": 2 * there + core},
-            device_id_type=MESH,
-        )
-
-    def both(turn, there):
-        at = pl.ds(pl.multiple_of((2 * there + core) * share, share), share)
-        return part_buf[turn, at, :].astype(F32) + half_buf[turn, there].astype(F32)
-
-    def product(turn):
-        source = owner(turn)
-        if turn >= ring:
-            for part in range(2):
-                heard_across(2, part, turn % ring)
-        at = pl.ds(pl.multiple_of(source * block, block), block)
-        part_buf[turn] = mm_nt(hidden[...], narrow_w[at, :]).astype(BF16)
-        for there in range(teams):
-            go(None, functools.partial(half_copy, turn, there))
-
-    def pass_on(turn):
-        for there in range(teams):
-            half_copy(turn, there).wait_recv()
-        for gap in range(1, teams):
-            there = lax.rem(line + gap, teams)
-            sum_buf[turn, there] = both(turn, there).astype(BF16)
-            go(None, functools.partial(far_copy, turn, there, line))
+    def far_copy(turn, ds, dl, heard):
+        group, there = chip(ds, dl)
+        slot = chip_at(ds, dl) if heard else chip_at(0, 0)
+        target = turn if heard or ds == 0 else turn + 1 - 2 * (turn % 2)
+        return pltpu.make_async_remote_copy(
+            src_ref=half_buf.at[turn, chip_at(ds, dl)],
+            dst_ref=far_buf.at[target, slot],
+            send_sem=far_send.at[turn, chip_at(ds, dl)],
+            recv_sem=far_recv.at[target, slot],
+            device_id={"sp": 2 * place + group, "tp": 2 * there + core},
+            device_id_type=MESH,
+        )
+
+    def both(turn, ds, dl):
+        mine = part_buf[rows_of(ds, dl, core), turn * block : (turn + 1) * block]
+        return mine.astype(F32) + half_buf[turn, chip_at(ds, dl)].astype(F32)
+
+    def source_of(turn):
+        return owner(nearest(ring, place, turn // 2), turn % 2)
+
+    def hear(part, gap):
+        if 0 < gap < ring and (part, gap) not in seen:
+            seen.add((part, gap))
+            arrive(2, part, gap)
+
+    def product(turn, ds, dl):
+        at = pl.ds(pl.multiple_of(source_of(turn) * block, block), block)
+        row = pl.ds(pl.multiple_of(chip_at(ds, dl) * tall, tall), tall)
+        part_buf[row, turn * block : (turn + 1) * block] = mm_nt(
+            hidden[row, :], narrow_w[at, :]
+        ).astype(BF16)
+        go(None, functools.partial(half_copy, turn, ds, dl))
+
+    def pass_on(turn, ds, dl):
+        half_copy(turn, ds, dl).wait_recv()
+        if (ds, dl) != (0, 0):
+            half_buf[turn, chip_at(ds, dl)] = both(turn, ds, dl).astype(BF16)
+            go(None, functools.partial(far_copy, turn, ds, dl, False))
 
     def close(turn):
-        col = pl.ds(pl.multiple_of(owner(turn) * block, block), block)
-        total = resid_buf[:, col] + both(turn, line)
-        for gap in range(1, teams):
-            there = lax.rem(line + gap, teams)
-            far_copy(turn, line, there).wait_recv()
-            total = total + far_buf[turn, there].astype(F32)
+        col = pl.ds(pl.multiple_of(source_of(turn) * block, block), block)
+        total = resid_buf[:, col] + both(turn, 0, 0)
+        for ds, dl in chips[1:]:
+            far_copy(turn, ds, dl, True).wait_recv()
+            total = total + far_buf[turn, chip_at(ds, dl)].astype(F32)
         out_buf[:, col] = total.astype(BF16)
         put(turn).start()
 
     def put(turn):
-        col = pl.ds(pl.multiple_of(owner(turn) * block, block), block)
+        col = pl.ds(pl.multiple_of(source_of(turn) * block, block), block)
         return pltpu.make_async_copy(out_buf.at[:, col], out_ref.at[:, col], out_sem.at[turn])
 
-    for turn in range(spread + 2):
-        if turn < spread:
-            product(turn)
-        if 1 <= turn <= spread:
-            pass_on(turn - 1)
-        if turn >= 2:
-            close(turn - 2)
+    farthest = sorted(chips, key=lambda c: (-(c[0] + (c[1] > 0)), c))
+    waiting = []
+    for count, (ds, dl) in enumerate(farthest):
+        hidden_rows(pl.multiple_of(chip_at(ds, dl) * tall, tall))
+        for one in waiting:
+            pass_on(*one)
+        waiting = [(turn, ds, dl) for turn in early_turns]
+        for one in waiting:
+            product(*one)
+        if count == 1:
+            hear(1, 1)
+        if count == len(chips) - 1:
+            hear(0, 2)
+    open_turns = list(early_turns)
+    for turn in range(len(early_turns), spread):
+        hear(turn % 2, turn // 2)
+        for ds, dl in farthest:
+            product(turn, ds, dl)
+        for one in waiting:
+            pass_on(*one)
+        waiting = [(turn, ds, dl) for ds, dl in farthest]
+        close(open_turns.pop(0))
+        open_turns.append(turn)
+    for one in waiting:
+        pass_on(*one)
+    for turn in open_turns:
+        close(turn)
     for turn in range(spread):
         put(turn).wait()
     for wanted, make in started:
@@ -566,11 +643,11 @@
     spread, team = lax.axis_size("sp"), lax.axis_size("tp")
     teams = team // 2
     length = q1.shape[0]
-    heads = v.shape[1] // LANES
+    heads = 2 * v.shape[2] // LANES
     chunks = length // CHUNK
     tiles = (q1.shape[1] + q2.shape[1]) // LANES
     share, width = skip.shape
-    block, units = gate.shape
+    block, units = gate.shape[0], gate.shape[1] // 2
     anywhere = pl.BlockSpec(memory_space=pl.ANY)
     inside = pl.BlockSpec(memory_space=pltpu.VMEM)
     dma = pltpu.SemaphoreType.DMA
@@ -583,6 +660,8 @@
         vmem(tiles, length, LANES),
         vmem(heads, length, LANES),
         vmem(heads, length, LANES),
+        vmem(*v.shape),
+        vmem(*v.shape),
         vmem(2 * heads, 1, length, dtype=F32),
         vmem(heads, length, LANES),
         vmem(heads, length, LANES, dtype=F32),
@@ -596,31 +675,29 @@
         vmem(*emis.shape),
         vmem(share, width),
         vmem(share, width, dtype=F32),
-        vmem(EDGE + length, width),
+        vmem(EDGE + 2 * length, width),
         vmem(width, units),
         vmem(width, units),
         vmem(width, units),
-        vmem(length, units),
-        vmem(spread, length, block),
-        vmem(spread, teams, share, block),
-        vmem(spread, teams, share, block),
-        vmem(spread, teams, share, block),
+        vmem(2 * length, units),
+        vmem(spread, 2 * teams, share, block),
+        vmem(spread, 2 * teams, share, block),
         vmem(share, width),
-        dma((2 * tiles + 2 * heads + 2,)),
+        dma((2 * tiles + 4,)),
         dma((3,)),
-        dma((3, spread, 2, 3)),
-        dma((3, spread, 2)),
+        dma((3, spread, 3)),
+        dma((3, spread)),
         dma((2,)),
         dma((2,)),
         dma((team,)),
         dma((team,)),
-        dma((2 * teams, 2)),
-        dma((team, 2)),
+        dma((2 * team, 2, 1 + teams)),
+        dma((2 * team, 2)),
         dma((2,)),
-        dma((spread, teams)),
-        dma((spread, teams)),
-        dma((spread, teams)),
-        dma((spread, teams)),
+        dma((spread, 2 * teams)),
+        dma((spread, 2 * teams)),
+        dma((spread, 2 * teams)),
+        dma((spread, 2 * teams)),
         dma((spread,)),
     ]
     return pl.pallas_call(
@@ -673,8 +750,8 @@
         former_match_vectors,
         jnp.pad(latter_request_vectors, ((0, 0), (0, spare))),
         jnp.pad(latter_match_vectors, ((0, 0), (0, spare))),
-        stored_vectors_both.reshape(length, -1),
-        closing_valve_operands.reshape(length, -1),
+        stored_vectors_both,
+        closing_valve_operands,
         emission_map_weights,
         arriving_hidden_state,
         switching_channel_map,

time: 240 us -> 202 us (0.84)
  Pallas kernels: 227 us -> 195 us
  local copies, waits for them, and re-layouts: 9.13 us -> 4.29 us
    pallas_call x1, Pallas kernels: 227 us -> 195 us  [whole_step(): pl.pallas_call(functools.partial(step_kernel, first), in_specs=[anywhere]...]
    unnamed x3 -> x1, local copies, waits for them, and re-layouts: 7.16 us -> 2.3 us
where the time goes in v1:
time: 202 us; the launch traced here: 201 us
  Pallas kernels  195 us (97%)
  local copies, waits for them, and re-layouts  4.29 us (2%)
    pallas_call x1, Pallas kernels, whole_step(): pl.pallas_call(functools.partial(step_kernel, first), in_specs=[anywhere]...  195 us

profile of v1, /device:TPU:28, one launch (start us, length us, event | category | flops | bytes accessed | tf_op | source)
XLA Modules:
  0.0 201.2 jit_solution(9439661356638479548)
XLA Ops:
  0.0 0.7 exponential_negate_fusion
  0.7 0.9 fusion.1
  1.6 0.6 reshape.17.gb_ref
  2.2 1.3 reshape.23.taps_ref
  3.6 195.4 %shard_map.181 = bf16[256,2048]{1,0:T(8,128)(2,1)} custom-call(bf16[1024,256]{1,0:T(8,128)(2,1)} %q1_ref.1, bf16[1024,256]{1,0:T(8,128)(2,1)} %k1_ref.1, bf16[1024,128]{1,0:T(8,128)(2,1)} %q2_ref.1, bf16[1024,128]{1,0:T(8,128)(2,1)} %k2_ref.1, bf16[1024,2,256]{2,1,0:T(2,128)(2,1)} %v_ref.1, bf16[1024,2,256]{2,1,0:T(2,128)(2,1)} %valve_ref.1, ...), custom_call_target="tpu_custom_call" | custom-call | flops 99999997952 | bytes 100000000 | tf_op jit(solution)/shard_map/pallas_call | solution.py:703
  198.9 2.3 %copy.21 = bf16[256,2048]{1,0:T(8,128)(2,1)} copy(bf16[256,2048]{1,0:T(8,128)(2,1)} %shard_map.181) | data formatting | bytes 2097152
  (1 shorter events, 0.0 us)
